TPU v7x, 32 devices: a whole 2x2x4 slice. The times are simulated.
32 devices in a mesh: sp: 8 (over z, x), tp: 4 (over y, core).
Axes of the slice: x: 2, y: 2, z: 4, core: 2. Of those that a mesh axis runs over, the one named last changes fastest.
Arguments:
- resid: bfloat16 [2048, 4096], P(('sp', 'tp')), may hold values from -6 to 6
- queries: bfloat16 [2048, 2048], P('sp', 'tp'), may hold values from -6 to 6
- keys: bfloat16 [2048, 512], P('sp', 'tp'), may hold values from -6 to 6
- values: bfloat16 [2048, 512], P('sp', 'tp'), may hold values from -6 to 6
- q_gain: float32 [128], replicated, may hold values from 0.5 to 6
- key_norm_gain: float32 [128], replicated, may hold values from 0.5 to 6
- out_weight: bfloat16 [2048, 4096], P('tp'), may hold values from -0.125 to 0.125
- norm1_gain: float32 [4096], replicated, may hold values from 0.1 to 1.9
- norm2_gain: float32 [4096], replicated, may hold values from 0.1 to 1.9
- expert_ids: int32 [2048, 2], P(('sp', 'tp')), may hold values from 0 to 7, all different within a row; in each aligned block of 64 rows (0 to 63, 64 to 127, ...) at most 24 rows name the same one
- group_weight: float32 [2048], P(('sp', 'tp')), may hold values from 0.3 to 1
- expert_weight: float32 [2048, 2], P(('sp', 'tp')), may hold values from 0.1 to 1
- gate_proj: bfloat16 [8, 4096, 1024], P('sp', None, 'tp'), may hold values from -0.09375 to 0.09375
- up_proj: bfloat16 [8, 4096, 1024], P('sp', None, 'tp'), may hold values from -0.09375 to 0.09375
- down_proj: bfloat16 [8, 1024, 4096], P('sp', 'tp'), may hold values from -0.1875 to 0.1875
Outputs:
- mixed_out: bfloat16 [2048, 4096], P(('sp', 'tp'))
Inputs may be any that keep to these rules, and one draw needn't show every extreme that they name: `expert_ids`: each row names 2 different experts. Among the rows of one device (aligned blocks of 64 rows) no expert is named by more than 24 rows, a bound that some block reaches.
All inputs are finite; a program needn't handle non-finite values.
Results may differ from a plain program's by a relative error of at most 0.012.
The roundings to bfloat16 on the way count: a program that leaves them out, or rounds other values in their place, can miss the bound.
Values may be sent and summed in bfloat16 or wider, within the bound.
A program may use at most 192 MiB of HBM per device.

v0:
```python
import functools

import jax
import jax.numpy as jnp
from jax import lax
from jax.experimental import pallas as pl
from jax.experimental.pallas import tpu as pltpu
from jax.sharding import PartitionSpec as P

GRID_W = 64


deep_alpha = 2.0**0.5
rope_theta = 10000.0


def apply_rotary_heads(block, gain, grid_positions):
    values32 = block.astype(jnp.float32)
    normed = values32 * lax.rsqrt(jnp.mean(values32 * values32, -1, keepdims=True) + 1e-06) * gain
    half = normed.shape[-1] // 2
    inv_freq = rope_theta ** (-jnp.arange(0, half, 2, dtype=jnp.float32) / half)
    grid_row = (grid_positions // GRID_W).astype(jnp.float32)
    grid_col = (grid_positions % GRID_W).astype(jnp.float32)
    angle = jnp.concatenate([grid_row[:, None] * inv_freq, grid_col[:, None] * inv_freq], -1)[
        :, None, :
    ]
    cosine = jnp.cos(angle)
    sine = jnp.sin(angle)
    first = normed[..., :half]
    second = normed[..., half:]
    turned = jnp.concatenate([first * cosine - second * sine, first * sine + second * cosine], -1)
    return turned.astype(jnp.bfloat16)


def layer_norm_gain(summed, gain):
    centre = summed - jnp.mean(summed, -1, keepdims=True)
    spread = jnp.mean(centre * centre, -1, keepdims=True)
    return centre * lax.rsqrt(spread + 1e-06) * gain


MESH = pl.DeviceIdType.MESH


def flip_bits(a, b, size):
    out = 0
    bit = 1
    while bit < size:
        out = out + ((a // bit + b // bit) % 2) * bit
        bit *= 2
    return out


def at_sp(index):
    return {"sp": index}


def at_tp(index):
    return {"tp": index}


def tp_partners(n_tp):
    t = lax.axis_index("tp")
    t1 = t + 1 - 2 * (t % 2)
    t2 = (t + n_tp // 2) % n_tp
    t3 = (t1 + n_tp // 2) % n_tp
    return t, t1, t2, t3


def attn_kernel(n_sp, heads, kv_heads, width, exponent_scale, q_ref, kv_ref, w_hbm, o_ref, slots, m_s, l_s, acc, attn, w, local, send, recv):
    me = lax.axis_index("sp")
    pair = me + 1 - 2 * (me % 2)
    group = heads // kv_heads
    load = pltpu.make_async_copy(w_hbm, w, local.at[0])
    load.start()

    barrier = pltpu.get_barrier_semaphore()
    pl.semaphore_signal(barrier, inc=1, device_id=at_sp(pair), device_id_type=MESH)

    def greet(j, _):
        pl.semaphore_signal(
            barrier, inc=1, device_id=at_sp(flip_bits(me, 2 * j, n_sp)), device_id_type=MESH
        )
        return 0

    lax.fori_loop(1, n_sp // 2, greet, 0)
    pl.semaphore_wait(barrier, n_sp // 2)

    def copy(src, slot, target):
        return pltpu.make_async_remote_copy(
            src_ref=src,
            dst_ref=slots.at[slot],
            send_sem=send.at[slot],
            recv_sem=recv.at[slot],
            device_id=at_sp(target),
            device_id_type=MESH,
        )

    copy(kv_ref, 1, pair).start()

    def spread(j, _):
        copy(kv_ref, 2 * j, flip_bits(me, 2 * j, n_sp)).start()
        return 0

    lax.fori_loop(1, n_sp // 2, spread, 0)

    m_s[...] = jnp.full(m_s.shape, -1e30, jnp.float32)
    l_s[...] = jnp.zeros(l_s.shape, jnp.float32)
    acc[...] = jnp.zeros(acc.shape, jnp.float32)

    def process(block):
        for h in range(heads):
            g = h // group
            q = q_ref[:, h * width : (h + 1) * width]
            k = block[:, g * width : (g + 1) * width]
            v = block[:, (kv_heads + g) * width : (kv_heads + g + 1) * width]
            s = lax.dot_general(q, k, (((1,), (1,)), ((), ())), preferred_element_type=jnp.float32)
            m_prev = m_s[h]
            m_new = jnp.maximum(m_prev, jnp.max(s, -1, keepdims=True))
            m_s[h] = m_new
            alpha = jnp.exp2((m_prev - m_new) * exponent_scale)
            p = jnp.exp2((s - m_new[:, :1]) * exponent_scale)
            l_s[h] = l_s[h] * alpha + jnp.sum(p, -1, keepdims=True)
            acc[h] = acc[h] * alpha + jnp.dot(
                p.astype(jnp.bfloat16), v, preferred_element_type=jnp.float32
            )

    process(kv_ref)

    def step(j, _):
        even = 2 * j + 2
        copy(kv_ref, even, pair).wait_recv()
        copy(slots.at[even], even + 1, pair).start()
        copy(kv_ref, even - 1, pair).wait_recv()
        process(slots.at[even - 1])
        process(slots.at[even])
        return 0

    lax.fori_loop(0, n_sp // 2 - 1, step, 0)
    copy(kv_ref, n_sp - 1, pair).wait_recv()
    process(slots.at[n_sp - 1])
    for h in range(heads):
        attn[:, h * width : (h + 1) * width] = (acc[h] / l_s[h]).astype(jnp.bfloat16)
    load.wait()
    columns = w.shape[1]
    strip = 512 if columns % 512 == 0 else columns
    for c in range(0, columns, strip):
        o_ref[:, c : c + strip] = jnp.dot(
            attn[...], w[:, c : c + strip], preferred_element_type=jnp.float32
        ).astype(jnp.bfloat16)

    def drain(slot, _):
        copy(kv_ref, slot, pair).wait_send()
        return 0

    lax.fori_loop(1, n_sp, drain, 0)


def attend(q_rot, kv, out_weight, n_sp, heads, kv_heads, width):
    rows = q_rot.shape[0]
    return pl.pallas_call(
        functools.partial(
            attn_kernel, n_sp, heads, kv_heads, width, width ** (-0.5) * 1.4426950408889634
        ),
        out_shape=jax.ShapeDtypeStruct((rows, out_weight.shape[1]), jnp.bfloat16),
        in_specs=[pl.BlockSpec(memory_space=pltpu.VMEM)] * 2 + [pl.BlockSpec(memory_space=pl.ANY)],
        out_specs=pl.BlockSpec(memory_space=pltpu.VMEM),
        scratch_shapes=[
            pltpu.VMEM((n_sp,) + kv.shape, jnp.bfloat16),
            pltpu.VMEM((heads, rows, 128), jnp.float32),
            pltpu.VMEM((heads, rows, 128), jnp.float32),
            pltpu.VMEM((heads, rows, width), jnp.float32),
            pltpu.VMEM((rows, heads * width), jnp.bfloat16),
            pltpu.VMEM(out_weight.shape, jnp.bfloat16),
            pltpu.SemaphoreType.DMA((1,)),
            pltpu.SemaphoreType.DMA((n_sp,)),
            pltpu.SemaphoreType.DMA((n_sp,)),
        ],
        compiler_params=pltpu.CompilerParams(collective_id=0, has_side_effects=True),
        name="attend",
    )(q_rot, kv, out_weight)


def moe_kernel(
    n_sp,
    n_tp,
    stride,
    out_ref,
    gate_hbm,
    up_hbm,
    down_hbm,
    back,
    w_gate,
    w_up,
    w_down,
    piece,
    rows,
    part,
    from_core,
    from_pair,
    pair_sum,
    total,
    local,
    send,
    recv,
):
    me = lax.axis_index("sp")
    t, t1, t2, t3 = tp_partners(n_tp)
    cap, width = out_ref.shape[1:]
    strip = 1024 if width % 1024 == 0 else width

    loads = [
        pltpu.make_async_copy(src, dst, local.at[i])
        for i, (src, dst) in enumerate(
            ((gate_hbm, w_gate), (up_hbm, w_up), (down_hbm, w_down), (out_ref.at[me], piece.at[me, t]))
        )
    ]
    for load in loads:
        load.start()

    barrier = pltpu.get_barrier_semaphore()
    pl.semaphore_signal(barrier, inc=1, device_id=at_tp(t1), device_id_type=MESH)
    pl.semaphore_signal(barrier, inc=1, device_id=at_tp(t2), device_id_type=MESH)

    def greet(k, _):
        pl.semaphore_signal(
            barrier, inc=1, device_id=at_sp(flip_bits(me, k, n_sp)), device_id_type=MESH
        )
        return 0

    lax.fori_loop(1, n_sp, greet, 0)
    pl.semaphore_wait(barrier, n_sp + 1)

    def order(i):
        return jnp.where(i < 2, i, 2 + (i - 2 + n_sp // 2 - 2) % max(n_sp - 2, 1))

    def copy(src, dst, kind, k, target):
        return pltpu.make_async_remote_copy(
            src_ref=src,
            dst_ref=dst,
            send_sem=send.at[kind, k],
            recv_sem=recv.at[kind, k],
            device_id=target,
            device_id_type=MESH,
        )

    def owner(k):
        return flip_bits(me, k, n_sp)

    def first_copy(k):
        return copy(out_ref.at[owner(k)], piece.at[me, t], 0, k, at_sp(owner(k)))

    def core_forward(k):
        return copy(piece.at[owner(k), t], piece.at[owner(k), t], 1, k, at_tp(t1))

    def pair_forward(k):
        return copy(piece.at[owner(k), t], piece.at[owner(k), t], 2, k, at_tp(t2))

    def relay_copy(k):
        return copy(piece.at[owner(k), t2], piece.at[owner(k), t2], 3, k, at_tp(t1))

    def core_part(k, half):
        lane = t3 if half else t1
        return copy(part.at[k, lane], from_core.at[k, half], 4 + half, k, at_tp(t1))

    def pair_part(k):
        return copy(pair_sum.at[k], from_pair.at[k], 6, k, at_tp(t2))

    def back_copy(k):
        return copy(total.at[k], back.at[me], 7, k, at_sp(owner(k)))

    copy(out_ref.at[me], piece.at[me, t], 2, 0, at_tp(t2)).start()
    copy(out_ref.at[me], piece.at[me, t], 1, 0, at_tp(t1)).start()

    def spread(i, _):
        first_copy(order(i)).start()
        return 0

    lax.fori_loop(1, n_sp, spread, 0)
    rows[...] = jnp.zeros(rows.shape, jnp.float32)
    for load in loads:
        load.wait()

    def stage_forward(k):
        first_copy(k).wait_recv()
        pair_forward(k).start()
        core_forward(k).start()

    def stage_relay(k):
        pair_forward(k).wait_recv()
        relay_copy(k).start()

    def stage_expert(k):
        core_forward(k).wait_recv()
        relay_copy(k).wait_recv()
        source = owner(k)
        for lane in range(n_tp):
            rows[lane * stride : lane * stride + cap, :] = piece[source, lane].astype(jnp.float32)
        gate = jnp.zeros((n_tp * stride, w_gate.shape[1]), jnp.float32)
        up = jnp.zeros((n_tp * stride, w_up.shape[1]), jnp.float32)
        for c in range(0, width, strip):
            x = rows[:, c : c + strip].astype(jnp.bfloat16)
            gate += jnp.dot(x, w_gate[c : c + strip, :], preferred_element_type=jnp.float32)
            up += jnp.dot(x, w_up[c : c + strip, :], preferred_element_type=jnp.float32)
        hidden = (gate / (1.0 + jnp.exp(-gate)) * up).astype(jnp.bfloat16)
        for c in range(0, width, strip):
            y = jnp.dot(hidden, w_down[:, c : c + strip], preferred_element_type=jnp.float32)
            for lane in range(n_tp):
                part[k, lane, :, c : c + strip] = y[lane * stride : lane * stride + cap].astype(
                    jnp.bfloat16
                )
        core_part(k, 1).start()
        core_part(k, 0).start()

    def stage_pair(k):
        core_part(k, 1).wait_recv()
        for c in range(0, width, strip):
            cols = slice(c, c + strip)
            pair_sum[k, :, cols] = (
                part[k, t2, :, cols].astype(jnp.float32)
                + from_core[k, 1, :, cols].astype(jnp.float32)
            ).astype(jnp.bfloat16)
        pair_part(k).start()

    def stage_total(k):
        core_part(k, 0).wait_recv()
        pair_part(k).wait_recv()

        def add(dst, row):
            for c in range(0, width, strip):
                cols = slice(c, c + strip)
                dst[row, :, cols] = (
                    part[k, t, :, cols].astype(jnp.float32)
                    + from_core[k, 0, :, cols].astype(jnp.float32)
                    + from_pair[k, :, cols].astype(jnp.float32)
                ).astype(jnp.bfloat16)

        @pl.when(k == 0)
        def _():
            add(back, me)

        @pl.when(k > 0)
        def _():
            add(total, k)
            back_copy(k).start()

    def tick(i, _):
        @pl.when(jnp.logical_and(i >= 1, i < n_sp))
        def _():
            stage_forward(order(i))

        @pl.when(jnp.logical_and(i >= 1, i < n_sp + 1))
        def _():
            stage_relay(order(i - 1))

        @pl.when(jnp.logical_and(i >= 2, i < n_sp + 2))
        def _():
            stage_pair(order(i - 2))

        @pl.when(i >= 3)
        def _():
            stage_total(order(i - 3))

        @pl.when(jnp.logical_and(i >= 1, i < n_sp + 1))
        def _():
            stage_expert(order(i - 1))

        return 0

    lax.fori_loop(0, n_sp + 3, tick, 0)

    def drain(k, _):
        core_forward(k).wait_send()
        pair_forward(k).wait_send()
        relay_copy(k).wait_send()
        core_part(k, 0).wait_send()
        core_part(k, 1).wait_send()
        pair_part(k).wait_send()
        return 0

    lax.fori_loop(0, n_sp, drain, 0)

    def drain_far(k, _):
        first_copy(k).wait_send()
        back_copy(k).wait()
        return 0

    lax.fori_loop(1, n_sp, drain_far, 0)


def experts(outgoing, gate_proj, up_proj, down_proj, n_sp, n_tp):
    block = outgoing.shape[1:]
    stride = (block[0] + 7) // 8 * 8
    slots = pltpu.VMEM((n_sp,) + block, jnp.bfloat16)
    lanes = pltpu.VMEM((n_sp, n_tp) + block, jnp.bfloat16)
    anywhere = pl.BlockSpec(memory_space=pl.ANY)
    return pl.pallas_call(
        functools.partial(moe_kernel, n_sp, n_tp, stride),
        out_shape=jax.ShapeDtypeStruct(outgoing.shape, jnp.bfloat16),
        in_specs=[pl.BlockSpec(memory_space=pltpu.VMEM), anywhere, anywhere, anywhere],
        out_specs=pl.BlockSpec(memory_space=pltpu.VMEM),
        scratch_shapes=[
            pltpu.VMEM(gate_proj.shape, jnp.bfloat16),
            pltpu.VMEM(up_proj.shape, jnp.bfloat16),
            pltpu.VMEM(down_proj.shape, jnp.bfloat16),
            lanes,
            pltpu.VMEM((n_tp * stride, block[1]), jnp.float32),
            lanes,
            pltpu.VMEM((n_sp, 2) + block, jnp.bfloat16),
            slots,
            slots,
            slots,
            pltpu.SemaphoreType.DMA((4,)),
            pltpu.SemaphoreType.DMA((8, n_sp)),
            pltpu.SemaphoreType.DMA((8, n_sp)),
        ],
        compiler_params=pltpu.CompilerParams(collective_id=1, has_side_effects=True),
        name="experts",
    )(outgoing, gate_proj, up_proj, down_proj)


def reduce_kernel(steps, n_tp, back, part, out, from_core, from_pair, pair_sum, total, send, recv):
    me = lax.axis_index("sp")
    t, t1, t2, t3 = tp_partners(n_tp)

    barrier = pltpu.get_barrier_semaphore()
    pl.semaphore_signal(barrier, inc=1, device_id=at_tp(t1), device_id_type=MESH)
    pl.semaphore_signal(barrier, inc=1, device_id=at_tp(t2), device_id_type=MESH)
    if back:

        def greet(k, _):
            pl.semaphore_signal(
                barrier, inc=1, device_id=at_sp(flip_bits(me, k, steps)), device_id_type=MESH
            )
            return 0

        lax.fori_loop(1, steps, greet, 0)
        pl.semaphore_wait(barrier, steps + 1)
    else:
        pl.semaphore_wait(barrier, 2)

    def order(i):
        return steps - 1 - i

    def block_of(k, lane):
        return flip_bits(me, k, steps) * n_tp + lane if back else lane * steps + k

    def copy(src, dst, kind, k, target):
        return pltpu.make_async_remote_copy(
            src_ref=src,
            dst_ref=dst,
            send_sem=send.at[kind, k],
            recv_sem=recv.at[kind, k],
            device_id=target,
            device_id_type=MESH,
        )

    def core_copy(k, half):
        lane = t3 if half else t1
        return copy(part.at[block_of(k, lane)], from_core.at[k, half], half, k, at_tp(t1))

    def pair_copy(k):
        return copy(pair_sum.at[k], from_pair.at[k], 2, k, at_tp(t2))

    def back_copy(k):
        return copy(total.at[k], out.at[me], 3, k, at_sp(flip_bits(me, k, steps)))

    def first(i, _):
        k = order(i)
        core_copy(k, 1).start()
        core_copy(k, 0).start()
        return 0

    lax.fori_loop(0, steps, first, 0)

    width = part.shape[-1]
    strip = 512 if width % 512 == 0 else width

    def add_pair(k):
        core_copy(k, 1).wait_recv()
        own = block_of(k, t2)
        for c in range(0, width, strip):
            cols = slice(c, c + strip)
            pair_sum[k, :, cols] = (
                part[own, :, cols].astype(jnp.float32)
                + from_core[k, 1, :, cols].astype(jnp.float32)
            ).astype(jnp.bfloat16)
        pair_copy(k).start()

    def add_all(k, dst, row):
        core_copy(k, 0).wait_recv()
        pair_copy(k).wait_recv()
        own = block_of(k, t)
        for c in range(0, width, strip):
            cols = slice(c, c + strip)
            dst[row, :, cols] = (
                part[own, :, cols].astype(jnp.float32)
                + from_core[k, 0, :, cols].astype(jnp.float32)
                + from_pair[k, :, cols].astype(jnp.float32)
            ).astype(jnp.bfloat16)

    def finish(k):
        if back:
            add_all(k, total, k)
            back_copy(k).start()
        else:
            add_all(k, out, k)

    depth = min(2, steps - 1)
    for i in range(depth):
        add_pair(order(i))

    def middle(i, _):
        add_pair(order(i))
        finish(order(i - depth))
        return 0

    lax.fori_loop(depth, steps, middle, 0)
    for i in range(steps - depth, steps - 1):
        finish(order(i))
    if back:
        add_all(0, out, me)
    else:
        finish(0)

    def drain(k, _):
        core_copy(k, 0).wait_send()
        core_copy(k, 1).wait_send()
        pair_copy(k).wait_send()
        return 0

    lax.fori_loop(0, steps, drain, 0)
    if back:

        def drain_back(k, _):
            back_copy(k).wait()
            return 0

        lax.fori_loop(1, steps, drain_back, 0)


def reduce_lanes(part, steps, n_tp, back, collective_id):
    block = part.shape[1:]
    slots = pltpu.VMEM((steps,) + block, jnp.bfloat16)
    return pl.pallas_call(
        functools.partial(reduce_kernel, steps, n_tp, back),
        out_shape=jax.ShapeDtypeStruct((steps,) + block, jnp.bfloat16),
        in_specs=[pl.BlockSpec(memory_space=pltpu.VMEM)],
        out_specs=pl.BlockSpec(memory_space=pltpu.VMEM),
        scratch_shapes=[
            pltpu.VMEM((steps, 2) + block, jnp.bfloat16),
            slots,
            slots,
            slots if back else pltpu.VMEM((1,) + block, jnp.bfloat16),
            pltpu.SemaphoreType.DMA((4, steps)),
            pltpu.SemaphoreType.DMA((4, steps)),
        ],
        compiler_params=pltpu.CompilerParams(collective_id=collective_id, has_side_effects=True),
        name="reduce_back" if back else "reduce_proj",
    )(part)


def per_device(
    resid,
    queries,
    keys,
    values,
    q_gain,
    key_norm_gain,
    out_weight,
    norm1_gain,
    norm2_gain,
    expert_ids,
    group_weight,
    expert_weight,
    gate_proj,
    up_proj,
    down_proj,
):
    local_tokens = queries.shape[0]
    head_size = q_gain.shape[0]
    kv_local = keys.shape[1] // head_size
    query_group = queries.shape[1] // head_size // kv_local
    model_width = resid.shape[1]
    grid_positions = lax.axis_index("sp") * local_tokens + jnp.arange(local_tokens, dtype=jnp.int32)
    q_rot = apply_rotary_heads(
        queries.reshape(local_tokens, kv_local * query_group, head_size), q_gain, grid_positions
    )
    q_rot = q_rot.reshape(local_tokens, kv_local * query_group * head_size)
    rotated_keys = apply_rotary_heads(
        keys.reshape(local_tokens, kv_local, head_size), key_norm_gain, grid_positions
    )
    rotated_keys = rotated_keys.reshape(local_tokens, kv_local * head_size)
    lanes = lax.axis_size("tp")
    sp_count = lax.axis_size("sp")
    own_rows = local_tokens // lanes
    kv = jnp.concatenate([rotated_keys, values], 1)
    proj_part = attend(
        q_rot, kv, out_weight, sp_count, kv_local * query_group, kv_local, head_size
    )
    proj_rows = 16
    proj_steps = own_rows // proj_rows
    proj = reduce_lanes(
        proj_part.reshape(lanes * proj_steps, proj_rows, model_width), proj_steps, lanes, False, 2
    )
    proj = proj.reshape(own_rows, model_width)
    summed = deep_alpha * resid.astype(jnp.float32) + proj.astype(jnp.float32)
    x_one = layer_norm_gain(summed, norm1_gain).astype(jnp.bfloat16)
    top_count = expert_ids.shape[1]
    expert_local = gate_proj.shape[0]
    expert_total = expert_local * sp_count
    capacity = (3 * top_count * own_rows + 2 * expert_total - 1) // (2 * expert_total)
    flat_ids = expert_ids.reshape(-1)
    one_hot = (flat_ids[:, None] == jnp.arange(expert_total, dtype=jnp.int32)[None, :]).astype(
        jnp.int32
    )
    earlier = jnp.cumsum(one_hot, 0) - one_hot
    rank = jnp.sum(earlier * one_hot, 1)
    slot = flat_ids * capacity + rank
    chosen = slot[:, None] == jnp.arange(expert_total * capacity, dtype=jnp.int32)[None, :]
    chosen = chosen.reshape(own_rows, top_count, expert_total * capacity)
    placing = jnp.sum(chosen.astype(jnp.bfloat16), 1)
    outgoing = lax.dot_general(
        placing, x_one, (((0,), (0,)), ((), ())), preferred_element_type=jnp.float32
    ).astype(jnp.bfloat16)
    outgoing = outgoing.reshape(expert_total, capacity, model_width)
    blocks = outgoing.reshape(sp_count, expert_local * capacity, model_width)
    returned = experts(
        blocks,
        gate_proj.reshape(gate_proj.shape[1:]),
        up_proj.reshape(up_proj.shape[1:]),
        down_proj.reshape(down_proj.shape[1:]),
        sp_count,
        lanes,
    )
    returned = returned.reshape(expert_total * capacity, model_width)
    gates = group_weight[:, None] * expert_weight / jnp.sum(expert_weight, -1, keepdims=True)
    combine = jnp.sum(jnp.where(chosen, gates[..., None], 0.0), 1)
    high = lax.reduce_precision(combine, 8, 7)
    both = jnp.concatenate([high, combine - high], 0).astype(jnp.bfloat16)
    picked = jnp.dot(both, returned, preferred_element_type=jnp.float32)
    moe = picked[:own_rows] + picked[own_rows:]
    final = deep_alpha * x_one.astype(jnp.float32) + moe
    return layer_norm_gain(final, norm2_gain).astype(jnp.bfloat16)


def solution(mesh):
    in_specs = (
        P(("sp", "tp"), None),
        P("sp", "tp"),
        P("sp", "tp"),
        P("sp", "tp"),
        P(),
        P(),
        P("tp", None),
        P(),
        P(),
        P(("sp", "tp"), None),
        P(("sp", "tp")),
        P(("sp", "tp"), None),
        P("sp", None, "tp"),
        P("sp", None, "tp"),
        P("sp", "tp", None),
    )
    out_specs = P(("sp", "tp"), None)
    return jax.shard_map(
        per_device, mesh=mesh, in_specs=in_specs, out_specs=out_specs, check_vma=False
    )
```

profile of v0, /device:TPU:9, one launch (start us, length us, event | category | flops | bytes accessed | tf_op | source)
XLA Modules:
  0.0 162.5 jit_solution(10921172110403608962)
XLA Ops:
  0.0 0.7 reduce_sum.101
  0.7 0.7 multiply_divide_fusion
  1.4 1.0 fusion.2
  2.4 0.8 copy.33
  4.0 0.7 multiply_add_fusion
  4.9 0.9 fusion.4
  6.0 0.6 fusion.7
  6.6 0.8 pad_maximum_fusion.3.kv_ref
  7.4 0.5 fusion.18
  8.1 0.3 multiply_reduce_fusion.2
  8.5 0.3 multiply_multiply_fusion
  8.9 0.5 subtract_convert_fusion
  9.4 0.4 pad_maximum_fusion
  9.7 0.7 copy.38
  10.5 23.2 %attend.1 = bf16[256,4096]{1,0:T(8,128)(2,1)} custom-call(bf16[256,512]{1,0:T(8,128)(2,1)} %bitcast.35, bf16[256,256]{1,0:T(8,128)(2,1)} %pad_maximum_fusion.3.kv_ref, bf16[512,4096]{1,0:T(8,128)(2,1)} %w_hbm.1), custom_call_target="tpu_custom_call" | custom-call | tf_op jit(solution)/shard_map/attend/pallas_call | solution.py:160
  33.7 21.0 %reduce_proj.1 = bf16[4,16,4096]{2,1,0:T(8,128)(2,1)} custom-call(bf16[16,16,4096]{2,1,0:T(8,128)(2,1)} %bitcast.28), custom_call_target="tpu_custom_call" | custom-call | tf_op jit(solution)/shard_map/reduce_proj/pallas_call | solution.py:544
  54.7 1.4 fusion.1
  56.1 1.4 multiply_reduce_fusion.1
  57.5 0.3 multiply_convert_fusion.1
  57.8 1.7 %convolution_convert_fusion = bf16[192,4096]{1,0:T(8,128)(2,1)} fusion(bf16[64,192]{1,0:T(8,128)(2,1)S(1)} %fusion.9, bf16[64,4096]{1,0:T(8,128)(2,1)S(1)} %multiply_convert_fusion.1), kind=kOutput, calls=%fused_computation | convolution fusion | flops 101449728 | bytes 2121728 | tf_op jit(solution)/shard_map/dot_general | solution.py:622
  59.5 99.5 %experts.1 = bf16[8,24,4096]{2,1,0:T(8,128)(2,1)} custom-call(bf16[8,24,4096]{2,1,0:T(8,128)(2,1)} %bitcast.30, bf16[4096,256]{1,0:T(8,128)(2,1)} %bitcast.31, bf16[4096,256]{1,0:T(8,128)(2,1)} %bitcast.32, bf16[256,4096]{1,0:T(8,128)(2,1)} %bitcast.33), custom_call_target="tpu_custom_call" | custom-call | tf_op jit(solution)/shard_map/experts/pallas_call | solution.py:396
  159.0 1.8 %fusion.10 = f32[128,4096]{1,0:T(8,128)S(1)} fusion(bf16[192,4096]{1,0:T(8,128)(2,1)} %bitcast.29, bf16[64,192]{1,0:T(8,128)(2,1)S(1)} %get-tuple-element.14, bf16[64,192]{1,0:T(8,128)(2,1)S(1)} %get-tuple-element.13), kind=kOutput, calls=%fused_computation.35 | convolution fusion | flops 201424896 | bytes 3719168 | tf_op jit(solution)/shard_map/dot_general | solution.py:640
  160.8 0.3 fusion.25
  161.5 1.0 multiply_convert_fusion
  (34 shorter events, 1.8 us)
Async XLA Ops:
  0.0 6.6 %copy-start.3 = (bf16[256,128]{1,0:T(8,128)(2,1)S(1)}, bf16[256,128]{1,0:T(8,128)(2,1)}, u32[]{:S(2)}) copy-start(bf16[256,128]{1,0:T(8,128)(2,1)} %param.18) | copy-start | bytes 196612
  0.0 7.9 %copy-start.2 = (bf16[256,512]{1,0:T(8,128)(2,1)S(1)}, bf16[256,512]{1,0:T(8,128)(2,1)}, u32[]{:S(2)}) copy-start(bf16[256,512]{1,0:T(8,128)(2,1)} %param.16) | copy-start | bytes 786436
  4.0 4.5 %copy-start.6 = (f32[128]{0:T(128)S(1)}, f32[128]{0:T(128)}, u32[]{:S(2)}) copy-start(f32[128]{0:T(128)} %param.19) | copy-start | bytes 1540
  33.6 21.0 %copy-start.1 = (bf16[64,4096]{1,0:T(8,128)(2,1)S(1)}, bf16[64,4096]{1,0:T(8,128)(2,1)}, u32[]{:S(2)}) copy-start(bf16[64,4096]{1,0:T(8,128)(2,1)} %param.15) | copy-start | bytes 1572868
  33.7 23.8 %copy-start.4 = (f32[4096]{0:T(1024)S(1)}, f32[4096]{0:T(1024)}, u32[]{:S(2)}) copy-start(f32[4096]{0:T(1024)} %param.22) | copy-start | bytes 49156
  54.7 2.8 %copy-start = (bf16[4,16,4096]{2,1,0:T(8,128)(2,1)S(1)}, bf16[4,16,4096]{2,1,0:T(8,128)(2,1)}, u32[]{:S(2)}) copy-start(bf16[4,16,4096]{2,1,0:T(8,128)(2,1)} %reduce_proj.1) | copy-start | bytes 1572868
  160.8 0.7 copy-start.5
where the time goes:
time: 163 us
  Pallas kernels  144 us (88%)
  other arithmetic  13 us (8%)
  matrix products  3.58 us (2%)
  local copies, waits for them, and re-layouts  2.14 us (1%)
    pallas_call x1, Pallas kernels, experts(): pl.pallas_call(functools.partial(moe_kernel, n_sp, n_tp, stride), out_sha...  99.5 us
    pallas_call x1, Pallas kernels, attend(): pl.pallas_call(functools.partial(attn_kernel, n_sp, heads, kv_heads, widt...  23.2 us
    pallas_call x1, Pallas kernels, reduce_lanes(): pl.pallas_call(functools.partial(reduce_kernel, steps, n_tp, back), out_s...  21 us

commit v1 on v0

v1 whole, which is shorter than its diff:
```python
import functools

import jax
import jax.numpy as jnp
import numpy as np
from jax import lax
from jax.experimental import pallas as pl
from jax.experimental.pallas import tpu as pltpu
from jax.sharding import PartitionSpec as P

GRID_W = 64


deep_alpha = 2.0**0.5
rope_theta = 10000.0


def rotation_table(tokens, half):
    freq = rope_theta ** (-np.arange(0, half, 2, dtype=np.float64) / half)
    blank = np.zeros((1, half // 2))
    rows = np.arange(tokens // GRID_W, dtype=np.float64)[:, None] * freq
    cols = np.arange(GRID_W, dtype=np.float64)[:, None] * freq

    def spread(angles, first):
        empty = np.broadcast_to(blank, angles.shape)
        place = (lambda v: [v, empty]) if first else (lambda v: [empty, v])
        cosine, sine = np.cos(angles), np.sin(angles)
        return [
            np.concatenate(place(cosine) + place(cosine), 1),
            np.concatenate(place(-sine) + place(sine), 1),
        ]

    return np.concatenate(spread(rows, True) + spread(cols, False), 0).astype(np.float32)


def rotate_block(block, gain, cosine, sine):
    values32 = block.astype(jnp.float32)
    normed = values32 * lax.rsqrt(jnp.mean(values32 * values32, -1, keepdims=True) + 1e-06) * gain
    half = normed.shape[-1] // 2
    return (normed * cosine + pltpu.roll(normed, half, 1) * sine).astype(jnp.bfloat16)


MESH = pl.DeviceIdType.MESH


def flip_bits(a, b, size):
    out = 0
    bit = 1
    while bit < size:
        out = out + ((a // bit + b // bit) % 2) * bit
        bit *= 2
    return out


def at_sp(index):
    return {"sp": index}


def at_tp(index):
    return {"tp": index}


def tp_partners(n_tp):
    t = lax.axis_index("tp")
    t1 = t + 1 - 2 * (t % 2)
    t2 = (t + n_tp // 2) % n_tp
    t3 = (t1 + n_tp // 2) % n_tp
    return t, t1, t2, t3


def attn_kernel(
    n_sp,
    n_tp,
    heads,
    kv_heads,
    width,
    cap,
    experts_total,
    exponent_scale,
    table,
    q_in,
    k_in,
    v_in,
    q_gain,
    k_gain,
    pack,
    gain,
    resid_hbm,
    w_hbm,
    down_hbm,
    x_out,
    outgoing,
    meta,
    down_cols,
    slots,
    q_ref,
    m_s,
    l_s,
    acc,
    attn,
    w,
    resid,
    place,
    part,
    from_core,
    from_pair,
    pair_sum,
    z,
    local,
    send,
    recv,
    sum_send,
    sum_recv,
    down_send,
    down_recv,
):
    me = lax.axis_index("sp")
    t, t1, t2, t3 = tp_partners(n_tp)
    pair = me + 1 - 2 * (me % 2)
    group = heads // kv_heads
    tokens = q_in.shape[0]
    strips, strip = w.shape[0], w.shape[2]
    own = z.shape[1]
    stride = (cap + 7) // 8 * 8

    def load(c):
        return pltpu.make_async_copy(
            w_hbm.at[:, pl.ds(pl.multiple_of(c * strip, strip), strip)], w.at[c], local.at[c]
        )

    def load_resid(c):
        return pltpu.make_async_copy(
            resid_hbm.at[:, pl.ds(pl.multiple_of(c * strip, strip), strip)],
            resid.at[c],
            local.at[strips + c],
        )

    def start_loads(c, _):
        load(c).start()
        load_resid(c).start()
        return 0

    lax.fori_loop(0, strips, start_loads, 0)

    barrier = pltpu.get_barrier_semaphore()
    pl.semaphore_signal(barrier, inc=1, device_id=at_sp(pair), device_id_type=MESH)
    pl.semaphore_signal(barrier, inc=1, device_id=at_tp(t1), device_id_type=MESH)
    pl.semaphore_signal(barrier, inc=1, device_id=at_tp(t2), device_id_type=MESH)
    pl.semaphore_signal(barrier, inc=1, device_id=at_tp(t3), device_id_type=MESH)

    def greet(j, _):
        pl.semaphore_signal(
            barrier, inc=1, device_id=at_sp(flip_bits(me, 2 * j, n_sp)), device_id_type=MESH
        )
        return 0

    lax.fori_loop(1, n_sp // 2, greet, 0)

    grid_rows = tokens // GRID_W
    all_rows = (table.shape[0] - 2 * GRID_W) // 2
    kv_ref = slots.at[0]

    def angles(i):
        row = me * grid_rows + i
        cosine = table[pl.ds(row, 1), :] + table[2 * all_rows : 2 * all_rows + GRID_W, :]
        sine = table[pl.ds(all_rows + row, 1), :] + table[2 * all_rows + GRID_W :, :]
        return cosine, sine

    for i in range(grid_rows):
        block = slice(i * GRID_W, (i + 1) * GRID_W)
        cosine, sine = angles(i)
        for g in range(kv_heads):
            lanes = slice(g * width, (g + 1) * width)
            kv_ref[block, lanes] = rotate_block(k_in[block, lanes], k_gain[...], cosine, sine)
    kv_ref[:, kv_heads * width :] = v_in[...]
    pl.semaphore_wait(barrier, n_sp // 2 + 3)

    def copy(src, slot, target):
        return pltpu.make_async_remote_copy(
            src_ref=src,
            dst_ref=slots.at[slot],
            send_sem=send.at[slot],
            recv_sem=recv.at[slot],
            device_id=at_sp(target),
            device_id_type=MESH,
        )

    copy(kv_ref, 1, pair).start()

    def spread(j, _):
        copy(kv_ref, 2 * j, flip_bits(me, 2 * j, n_sp)).start()
        return 0

    lax.fori_loop(1, n_sp // 2, spread, 0)

    share = down_cols.shape[2]

    def down_copy(j):
        target = (t1, t2, t3)[j]
        return pltpu.make_async_remote_copy(
            src_ref=down_hbm.at[:, pl.ds(pl.multiple_of(target * share, share), share)],
            dst_ref=down_cols.at[t],
            send_sem=down_send.at[j],
            recv_sem=down_recv.at[j],
            device_id=at_tp(target),
            device_id_type=MESH,
        )

    for j in range(3):
        down_copy(j).start()

    for i in range(grid_rows):
        block = slice(i * GRID_W, (i + 1) * GRID_W)
        cosine, sine = angles(i)
        for h in range(heads):
            lanes = slice(h * width, (h + 1) * width)
            q_ref[block, lanes] = rotate_block(q_in[block, lanes], q_gain[...], cosine, sine)

    m_s[...] = jnp.full(m_s.shape, -1e30, jnp.float32)
    l_s[...] = jnp.zeros(l_s.shape, jnp.float32)
    acc[...] = jnp.zeros(acc.shape, jnp.float32)

    def process(block):
        for h in range(heads):
            g = h // group
            q = q_ref[:, h * width : (h + 1) * width]
            k = block[:, g * width : (g + 1) * width]
            v = block[:, (kv_heads + g) * width : (kv_heads + g + 1) * width]
            s = lax.dot_general(q, k, (((1,), (1,)), ((), ())), preferred_element_type=jnp.float32)
            m_prev = m_s[h]
            m_new = jnp.maximum(m_prev, jnp.max(s, -1, keepdims=True))
            m_s[h] = m_new
            alpha = jnp.exp2((m_prev - m_new) * exponent_scale)
            p = jnp.exp2((s - m_new[:, :1]) * exponent_scale)
            l_s[h] = l_s[h] * alpha + jnp.sum(p, -1, keepdims=True)
            acc[h] = acc[h] * alpha + jnp.dot(
                p.astype(jnp.bfloat16), v, preferred_element_type=jnp.float32
            )

    process(kv_ref)

    lane = lax.broadcasted_iota(jnp.int32, (own, 128), 1).astype(jnp.float32)
    e0, e1 = pack[:, 0:1], pack[:, 1:2]
    named0 = jnp.where(lane == e0, 1.0, 0.0)
    named1 = jnp.where(lane == e1, 1.0, 0.0)
    before = (
        lax.broadcasted_iota(jnp.int32, (own, own), 0)
        > lax.broadcasted_iota(jnp.int32, (own, own), 1)
    )
    before = jnp.where(before, 1.0, 0.0).astype(jnp.bfloat16)
    earlier = jnp.dot(
        before, (named0 + named1).astype(jnp.bfloat16), preferred_element_type=jnp.float32
    )
    slot0 = e0 * stride + jnp.sum(earlier * named0, -1, keepdims=True)
    slot1 = e1 * stride + jnp.sum(earlier * named1, -1, keepdims=True)
    column = lax.broadcasted_iota(jnp.int32, place.shape, 1).astype(jnp.float32)
    place[...] = jnp.where(
        column == slot0, 1.0, jnp.where(column == slot1, 1.0, 0.0)
    ).astype(jnp.bfloat16)
    meta[...] = jnp.where(
        lane == 0.0,
        slot0,
        jnp.where(lane == 1.0, slot1, jnp.where(lane == 2.0, pack[:, 2:3], pack[:, 3:4])),
    )

    def step(j, _):
        even = 2 * j + 2
        copy(kv_ref, even, pair).wait_recv()
        copy(slots.at[even], even + 1, pair).start()
        copy(kv_ref, even - 1, pair).wait_recv()
        process(slots.at[even - 1])
        process(slots.at[even])
        return 0

    lax.fori_loop(0, n_sp // 2 - 1, step, 0)
    copy(kv_ref, n_sp - 1, pair).wait_recv()
    process(slots.at[n_sp - 1])
    for h in range(heads):
        attn[:, h * width : (h + 1) * width] = (acc[h] / l_s[h]).astype(jnp.bfloat16)

    def sum_copy(src, dst, kind, c, target):
        return pltpu.make_async_remote_copy(
            src_ref=src,
            dst_ref=dst,
            send_sem=sum_send.at[kind, c],
            recv_sem=sum_recv.at[kind, c],
            device_id=at_tp(target),
            device_id_type=MESH,
        )

    def core_copy(c, half):
        return sum_copy(part.at[c, t3 if half else t1], from_core.at[c, half], half, c, t1)

    def pair_copy(c):
        return sum_copy(pair_sum.at[c], from_pair.at[c], 2, c, t2)

    def project(c):
        load(c).wait()
        y = jnp.dot(attn[...], w[c], preferred_element_type=jnp.float32)
        for i in range(n_tp):
            part[c, i] = y[i * own : (i + 1) * own].astype(jnp.bfloat16)
        core_copy(c, 1).start()
        core_copy(c, 0).start()

    def add_pair(c):
        core_copy(c, 1).wait_recv()
        pair_sum[c] = (
            part[c, t2].astype(jnp.float32) + from_core[c, 1].astype(jnp.float32)
        ).astype(jnp.bfloat16)
        pair_copy(c).start()

    depth = min(4, strips)

    def reduce_step(c, _):
        @pl.when(c < strips)
        def _():
            project(c)

        @pl.when(c >= depth)
        def _():
            add_pair(c - depth)

        return 0

    lax.fori_loop(0, strips + depth, reduce_step, 0)

    def finish(c, total):
        core_copy(c, 0).wait_recv()
        pair_copy(c).wait_recv()
        load_resid(c).wait()
        proj = (
            part[c, t].astype(jnp.float32)
            + from_core[c, 0].astype(jnp.float32)
            + from_pair[c].astype(jnp.float32)
        ).astype(jnp.bfloat16)
        summed = deep_alpha * resid[c].astype(jnp.float32) + proj.astype(jnp.float32)
        z[c] = summed
        return total + jnp.sum(summed, -1, keepdims=True)

    features = strips * strip
    mean = lax.fori_loop(0, strips, finish, jnp.zeros((own, 1), jnp.float32)) / features

    def deviate(c, total):
        centre = z[c] - mean
        return total + jnp.sum(centre * centre, -1, keepdims=True)

    spread_sum = lax.fori_loop(0, strips, deviate, jnp.zeros((own, 1), jnp.float32))
    scale = lax.rsqrt(spread_sum / features + 1e-06)

    for c in range(strips):
        cols = slice(c * strip, (c + 1) * strip)
        x = ((z[c] - mean) * scale * gain[:, cols]).astype(jnp.bfloat16)
        x_out[:, cols] = x
        rows = lax.dot_general(
            place[...], x, (((0,), (0,)), ((), ())), preferred_element_type=jnp.float32
        )
        for e in range(experts_total):
            outgoing[e, :, cols] = rows[e * stride : e * stride + cap].astype(jnp.bfloat16)

    def drain(slot, _):
        copy(kv_ref, slot, pair).wait_send()
        return 0

    lax.fori_loop(1, n_sp, drain, 0)

    def drain_sum(c, _):
        core_copy(c, 0).wait_send()
        core_copy(c, 1).wait_send()
        pair_copy(c).wait_send()
        return 0

    lax.fori_loop(0, strips, drain_sum, 0)
    for j in range(3):
        down_copy(j).wait()


def attend(
    queries,
    keys,
    values,
    q_gain,
    k_gain,
    pack,
    gain,
    resid,
    out_weight,
    down_proj,
    n_sp,
    n_tp,
    experts_total,
    cap,
):
    tokens, q_width = queries.shape
    width = q_gain.shape[-1]
    heads, kv_heads = q_width // width, keys.shape[1] // width
    own, features = resid.shape
    strip = 512 if features % 512 == 0 else features
    strips = features // strip
    stride = (cap + 7) // 8 * 8
    table = rotation_table(tokens * n_sp, width // 2)
    chunk = (strips, own, strip)
    vmem = pl.BlockSpec(memory_space=pltpu.VMEM)
    anywhere = pl.BlockSpec(memory_space=pl.ANY)
    return pl.pallas_call(
        functools.partial(
            attn_kernel,
            n_sp,
            n_tp,
            heads,
            kv_heads,
            width,
            cap,
            experts_total,
            width ** (-0.5) * 1.4426950408889634,
        ),
        out_shape=(
            jax.ShapeDtypeStruct((own, features), jnp.bfloat16),
            jax.ShapeDtypeStruct((experts_total, cap, features), jnp.bfloat16),
            jax.ShapeDtypeStruct((own, 128), jnp.float32),
            jax.ShapeDtypeStruct((n_tp, down_proj.shape[0], features // n_tp), jnp.bfloat16),
        ),
        in_specs=[vmem] * 8 + [anywhere] * 3,
        out_specs=(vmem, vmem, vmem, anywhere),
        scratch_shapes=[
            pltpu.VMEM((n_sp, tokens, 2 * kv_heads * width), jnp.bfloat16),
            pltpu.VMEM((tokens, q_width), jnp.bfloat16),
            pltpu.VMEM((heads, tokens, 128), jnp.float32),
            pltpu.VMEM((heads, tokens, 128), jnp.float32),
            pltpu.VMEM((heads, tokens, width), jnp.float32),
            pltpu.VMEM((tokens, q_width), jnp.bfloat16),
            pltpu.VMEM((strips, out_weight.shape[0], strip), jnp.bfloat16),
            pltpu.VMEM(chunk, jnp.bfloat16),
            pltpu.VMEM((own, experts_total * stride), jnp.bfloat16),
            pltpu.VMEM((strips, n_tp, own, strip), jnp.bfloat16),
            pltpu.VMEM((strips, 2, own, strip), jnp.bfloat16),
            pltpu.VMEM(chunk, jnp.bfloat16),
            pltpu.VMEM(chunk, jnp.bfloat16),
            pltpu.VMEM(chunk, jnp.float32),
            pltpu.SemaphoreType.DMA((2 * strips,)),
            pltpu.SemaphoreType.DMA((n_sp,)),
            pltpu.SemaphoreType.DMA((n_sp,)),
            pltpu.SemaphoreType.DMA((3, strips)),
            pltpu.SemaphoreType.DMA((3, strips)),
            pltpu.SemaphoreType.DMA((3,)),
            pltpu.SemaphoreType.DMA((3,)),
        ],
        compiler_params=pltpu.CompilerParams(collective_id=0, has_side_effects=True),
        name="attend",
    )(jnp.asarray(table), queries, keys, values, q_gain, k_gain, pack, gain, resid, out_weight, down_proj)


def moe_kernel(
    n_sp,
    n_tp,
    stride,
    out_ref,
    meta,
    x_one,
    gain,
    gate_hbm,
    up_hbm,
    down_hbm,
    down_cols,
    final,
    w_gate,
    w_up,
    w_down,
    piece,
    rows,
    hidden,
    answer,
    back,
    metas,
    moe,
    moe_send,
    moe_recv,
    local,
    send,
    recv,
    small_send,
    small_recv,
):
    me = lax.axis_index("sp")
    t, t1, t2, t3 = tp_partners(n_tp)
    peers = (t1, t2, t3)
    cap, width = out_ref.shape[1:]
    strip = 1024 if width % 1024 == 0 else width
    share = w_down.shape[2]
    own = final.shape[0]

    loads = [
        pltpu.make_async_copy(src, dst, local.at[i])
        for i, (src, dst) in enumerate(
            (
                (out_ref.at[me], piece.at[me, t]),
                (gate_hbm, w_gate),
                (up_hbm, w_up),
                (down_hbm.at[:, pl.ds(pl.multiple_of(t * share, share), share)], w_down.at[t]),
                (down_cols.at[t1], w_down.at[t1]),
                (down_cols.at[t2], w_down.at[t2]),
                (down_cols.at[t3], w_down.at[t3]),
            )
        )
    ]
    for load in loads:
        load.start()

    barrier = pltpu.get_barrier_semaphore()
    for peer in peers:
        pl.semaphore_signal(barrier, inc=1, device_id=at_tp(peer), device_id_type=MESH)

    def greet(k, _):
        pl.semaphore_signal(
            barrier, inc=1, device_id=at_sp(flip_bits(me, k, n_sp)), device_id_type=MESH
        )
        return 0

    lax.fori_loop(1, n_sp, greet, 0)
    pl.semaphore_wait(barrier, n_sp + 2)

    def order(i):
        return jnp.where(i < 2, i, 2 + (i - 2 + n_sp // 2 - 2) % max(n_sp - 2, 1))

    def copy(src, dst, kind, k, target):
        return pltpu.make_async_remote_copy(
            src_ref=src,
            dst_ref=dst,
            send_sem=send.at[kind, k],
            recv_sem=recv.at[kind, k],
            device_id=target,
            device_id_type=MESH,
        )

    def owner(k):
        return flip_bits(me, k, n_sp)

    def first_copy(k):
        return copy(out_ref.at[owner(k)], piece.at[me, t], 0, k, at_sp(owner(k)))

    def core_forward(k):
        return copy(piece.at[owner(k), t], piece.at[owner(k), t], 1, k, at_tp(t1))

    def pair_forward(k):
        return copy(piece.at[owner(k), t], piece.at[owner(k), t], 2, k, at_tp(t2))

    def relay_copy(k):
        return copy(piece.at[owner(k), t2], piece.at[owner(k), t2], 3, k, at_tp(t1))

    def hidden_copy(k, j):
        return copy(hidden.at[k, t], hidden.at[k, t], 4 + j, k, at_tp(peers[j]))

    def back_copy(k):
        return copy(answer.at[k], back.at[me], 7, k, at_sp(owner(k)))

    def small_copy(src, dst, kind, j):
        return pltpu.make_async_remote_copy(
            src_ref=src,
            dst_ref=dst,
            send_sem=small_send.at[kind, j],
            recv_sem=small_recv.at[kind, j],
            device_id=at_tp(peers[j]),
            device_id_type=MESH,
        )

    def meta_copy(j):
        return small_copy(meta, metas.at[t], 0, j)

    def moe_copy(j):
        return small_copy(moe_send.at[peers[j]], moe_recv.at[t], 1, j)

    copy(out_ref.at[me], piece.at[me, t], 2, 0, at_tp(t2)).start()
    copy(out_ref.at[me], piece.at[me, t], 1, 0, at_tp(t1)).start()

    def spread(i, _):
        first_copy(order(i)).start()
        return 0

    lax.fori_loop(1, n_sp, spread, 0)
    for j in range(3):
        meta_copy(j).start()
    metas[t] = meta[...]
    rows[...] = jnp.zeros(rows.shape, jnp.float32)
    moe[...] = jnp.zeros(moe.shape, jnp.float32)
    for load in loads:
        load.wait()

    def stage_forward(k):
        first_copy(k).wait_recv()
        pair_forward(k).start()
        core_forward(k).start()

    def stage_relay(k):
        pair_forward(k).wait_recv()
        relay_copy(k).start()

    def stage_expert(k):
        core_forward(k).wait_recv()
        relay_copy(k).wait_recv()
        source = owner(k)
        for lane in range(n_tp):
            rows[lane * stride : lane * stride + cap, :] = piece[source, lane].astype(jnp.float32)
        gate = jnp.zeros((n_tp * stride, w_gate.shape[1]), jnp.float32)
        up = jnp.zeros((n_tp * stride, w_up.shape[1]), jnp.float32)
        for c in range(0, width, strip):
            x = rows[:, c : c + strip].astype(jnp.bfloat16)
            gate += jnp.dot(x, w_gate[c : c + strip, :], preferred_element_type=jnp.float32)
            up += jnp.dot(x, w_up[c : c + strip, :], preferred_element_type=jnp.float32)
        hidden[k, t] = (gate / (1.0 + jnp.exp(-gate)) * up).astype(jnp.bfloat16)
        for j in (1, 2, 0):
            hidden_copy(k, j).start()

    def stage_down(k):
        for j in range(3):
            hidden_copy(k, j).wait_recv()
        y = jnp.zeros((n_tp * stride, share), jnp.float32)
        for s in range(n_tp):
            y += jnp.dot(hidden[k, s], w_down[s], preferred_element_type=jnp.float32)

        def put(dst, row):
            for lane in range(n_tp):
                dst[row, lane] = y[lane * stride : lane * stride + cap].astype(jnp.bfloat16)

        @pl.when(k == 0)
        def _():
            put(back, me)

        @pl.when(k > 0)
        def _():
            put(answer, k)
            back_copy(k).start()

    def tick(i, _):
        @pl.when(jnp.logical_and(i >= 1, i < n_sp))
        def _():
            stage_forward(order(i))

        @pl.when(jnp.logical_and(i >= 1, i < n_sp + 1))
        def _():
            stage_relay(order(i - 1))

        @pl.when(i >= 2)
        def _():
            stage_down(order(i - 2))

        @pl.when(jnp.logical_and(i >= 1, i < n_sp + 1))
        def _():
            stage_expert(order(i - 1))

        return 0

    lax.fori_loop(0, n_sp + 2, tick, 0)

    for j in range(3):
        meta_copy(j).wait_recv()

    column = lax.broadcasted_iota(jnp.int32, (own, n_tp * stride), 1).astype(jnp.float32)

    def gather(k):
        source = owner(k)
        for lane in range(n_tp):
            rows[lane * stride : lane * stride + cap, :share] = back[source, lane].astype(
                jnp.float32
            )
        return rows[:, :share].astype(jnp.bfloat16), source

    def weigh(taken, source, lane):
        about = metas[lane]
        low = (source * stride).astype(jnp.float32)
        shift = ((lane - source) * stride).astype(jnp.float32)
        weight = jnp.zeros(column.shape, jnp.float32)
        for choice in range(2):
            slot = about[:, choice : choice + 1]
            inside = jnp.logical_and(slot >= low, slot < low + stride)
            target = jnp.where(inside, slot + shift, -1.0)
            weight += jnp.where(column == target, about[:, 2 + choice : 3 + choice], 0.0)
        high = weight.astype(jnp.bfloat16)
        low_part = (weight - high.astype(jnp.float32)).astype(jnp.bfloat16)
        both = jnp.concatenate([high, low_part], 0)
        picked = jnp.dot(both, taken, preferred_element_type=jnp.float32)
        return moe[lane] + (picked[:own] + picked[own:])

    def combine(i, _):
        k = order(i)

        @pl.when(k > 0)
        def _():
            back_copy(k).wait_recv()

        taken, source = gather(k)
        for lane in range(n_tp):
            moe[lane] = weigh(taken, source, lane)
        return 0

    lax.fori_loop(0, n_sp - 1, combine, 0)
    last = order(n_sp - 1)
    back_copy(last).wait_recv()
    taken, source = gather(last)
    for j in (1, 2, 0):
        moe_send[peers[j]] = weigh(taken, source, peers[j]).astype(jnp.bfloat16)
        moe_copy(j).start()
    mine = weigh(taken, source, t)

    def add(lane, value):
        cols = pl.ds(pl.multiple_of(lane * share, share), share)
        summed = deep_alpha * x_one[:, cols].astype(jnp.float32) + value
        moe[lane] = summed
        return jnp.sum(summed, -1, keepdims=True)

    total = add(t, mine)
    for j in range(3):
        moe_copy(j).wait_recv()
        total += add(peers[j], moe_recv[peers[j]].astype(jnp.float32))
    mean = total / width
    spread_sum = jnp.zeros((own, 1), jnp.float32)
    for s in range(n_tp):
        centre = moe[s] - mean
        spread_sum += jnp.sum(centre * centre, -1, keepdims=True)
    scale = lax.rsqrt(spread_sum / width + 1e-06)
    for s in range(n_tp):
        cols = slice(s * share, (s + 1) * share)
        final[:, cols] = ((moe[s] - mean) * scale * gain[:, cols]).astype(jnp.bfloat16)

    def drain(k, _):
        core_forward(k).wait_send()
        pair_forward(k).wait_send()
        relay_copy(k).wait_send()
        for j in range(3):
            hidden_copy(k, j).wait_send()
        return 0

    lax.fori_loop(0, n_sp, drain, 0)

    def drain_far(k, _):
        first_copy(k).wait_send()
        back_copy(k).wait_send()
        return 0

    lax.fori_loop(1, n_sp, drain_far, 0)
    for j in range(3):
        meta_copy(j).wait_send()
        moe_copy(j).wait_send()


def experts(outgoing, meta, x_one, gain, gate_proj, up_proj, down_proj, down_cols, n_sp, n_tp):
    cap, features = outgoing.shape[1:]
    stride = (cap + 7) // 8 * 8
    own = x_one.shape[0]
    share = features // n_tp
    hidden_share = gate_proj.shape[1]
    vmem = pl.BlockSpec(memory_space=pltpu.VMEM)
    anywhere = pl.BlockSpec(memory_space=pl.ANY)
    slots = pltpu.VMEM((n_sp, n_tp, cap, share), jnp.bfloat16)
    split = pltpu.VMEM((n_tp, own, share), jnp.bfloat16)
    return pl.pallas_call(
        functools.partial(moe_kernel, n_sp, n_tp, stride),
        out_shape=jax.ShapeDtypeStruct((own, features), jnp.bfloat16),
        in_specs=[vmem] * 4 + [anywhere] * 4,
        out_specs=vmem,
        scratch_shapes=[
            pltpu.VMEM(gate_proj.shape, jnp.bfloat16),
            pltpu.VMEM(up_proj.shape, jnp.bfloat16),
            pltpu.VMEM(down_cols.shape, jnp.bfloat16),
            pltpu.VMEM((n_sp, n_tp, cap, features), jnp.bfloat16),
            pltpu.VMEM((n_tp * stride, features), jnp.float32),
            pltpu.VMEM((n_sp, n_tp, n_tp * stride, hidden_share), jnp.bfloat16),
            slots,
            slots,
            pltpu.VMEM((n_tp,) + meta.shape, jnp.float32),
            pltpu.VMEM((n_tp, own, share), jnp.float32),
            split,
            split,
            pltpu.SemaphoreType.DMA((7,)),
            pltpu.SemaphoreType.DMA((8, n_sp)),
            pltpu.SemaphoreType.DMA((8, n_sp)),
            pltpu.SemaphoreType.DMA((2, 3)),
            pltpu.SemaphoreType.DMA((2, 3)),
        ],
        compiler_params=pltpu.CompilerParams(collective_id=1, has_side_effects=True),
        name="experts",
    )(outgoing, meta, x_one, gain, gate_proj, up_proj, down_proj, down_cols)


def per_device(
    resid,
    queries,
    keys,
    values,
    q_gain,
    key_norm_gain,
    out_weight,
    norm1_gain,
    norm2_gain,
    expert_ids,
    group_weight,
    expert_weight,
    gate_proj,
    up_proj,
    down_proj,
):
    lanes = lax.axis_size("tp")
    sp_count = lax.axis_size("sp")
    own_rows, model_width = resid.shape
    top_count = expert_ids.shape[1]
    expert_local = gate_proj.shape[0]
    expert_total = expert_local * sp_count
    capacity = (3 * top_count * own_rows + 2 * expert_total - 1) // (2 * expert_total)
    gates = group_weight[:, None] * expert_weight / jnp.sum(expert_weight, -1, keepdims=True)
    pack = jnp.concatenate([expert_ids.astype(jnp.float32), gates], 1)
    down_local = down_proj.reshape(down_proj.shape[1:])
    x_one, outgoing, meta, down_cols = attend(
        queries,
        keys,
        values,
        q_gain[None, :],
        key_norm_gain[None, :],
        pack,
        norm1_gain[None, :],
        resid,
        out_weight,
        down_local,
        sp_count,
        lanes,
        expert_total,
        capacity,
    )
    return experts(
        outgoing.reshape(sp_count, expert_local * capacity, model_width),
        meta,
        x_one,
        norm2_gain[None, :],
        gate_proj.reshape(gate_proj.shape[1:]),
        up_proj.reshape(up_proj.shape[1:]),
        down_local,
        down_cols,
        sp_count,
        lanes,
    )


def solution(mesh):
    in_specs = (
        P(("sp", "tp"), None),
        P("sp", "tp"),
        P("sp", "tp"),
        P("sp", "tp"),
        P(),
        P(),
        P("tp", None),
        P(),
        P(),
        P(("sp", "tp"), None),
        P(("sp", "tp")),
        P(("sp", "tp"), None),
        P("sp", None, "tp"),
        P("sp", None, "tp"),
        P("sp", "tp", None),
    )
    out_specs = P(("sp", "tp"), None)
    return jax.shard_map(
        per_device, mesh=mesh, in_specs=in_specs, out_specs=out_specs, check_vma=False
    )
```

time: 163 us -> 138 us (0.85)
  Pallas kernels: 144 us -> 133 us
  other arithmetic: 13 us -> 2.08 us
  matrix products: 3.58 us -> 0 us
    pallas_call x1, Pallas kernels: 99.5 us -> 90.4 us  [experts(): pl.pallas_call(functools.partial(moe_kernel, n_sp, n_tp, stride), out_sha...]
    reduce_sum x9 -> x0, other arithmetic: 5.01 us -> none  [the longest x2 1.69 us: layer_norm_gain(): centre = summed - jnp.mean(summed, -1, keepdims=True)]
    dot_general x2 -> x0, matrix products: 3.58 us -> none  [the longest x1 1.84 us: per_device(): picked = jnp.dot(both, returned, preferred_element_type=jnp.float32)]
    concatenate x4 -> x1, other arithmetic: 1.84 us -> 0.01 us  [per_device(): pack = jnp.concatenate([expert_ids.astype(jnp.float32), gates], 1)]
    pallas_call x2 -> x1, Pallas kernels: 44.1 us -> 42.4 us  [attend(): pl.pallas_call(functools.partial(attn_kernel, n_sp, n_tp, heads, kv_heads...]
where the time goes in v1:
time: 138 us
  Pallas kernels  133 us (96%)
  local copies, waits for them, and re-layouts  2.58 us (2%)
  other arithmetic  2.08 us (2%)
    pallas_call x1, Pallas kernels, experts(): pl.pallas_call(functools.partial(moe_kernel, n_sp, n_tp, stride), out_sha...  90.4 us
    pallas_call x1, Pallas kernels, attend(): pl.pallas_call(functools.partial(attn_kernel, n_sp, n_tp, heads, kv_heads...  42.4 us

profile of v1, /device:TPU:9, one launch (start us, length us, event | category | flops | bytes accessed | tf_op | source)
XLA Modules:
  0.0 137.5 jit_solution(7944214276518743258)
XLA Ops:
  0.0 0.7 reduce_sum.9
  0.7 0.7 multiply_divide_fusion
  1.4 0.7 convert_element_type.3
  2.1 0.7 copy.21.pack
  2.8 42.4 %attend.1 = (bf16[64,4096]{1,0:T(8,128)(2,1)}, bf16[8,24,4096]{2,1,0:T(8,128)(2,1)}, f32[64,128]{1,0:T(8,128)}, bf16[4,256,1024]{2,1,0:T(8,128)(2,1)}) custom-call(f32[192,128]{1,0:T(8,128)} %constant.4.clone.table, bf16[256,512]{1,0:T(8,128)(2,1)} %q_in.1, bf16[256,128]{1,0:T(8,128)(2,1)} %k_in.1, bf16[256,128]{1,0:T(8,128)(2,1)} %v_in.1, ...), custom_call_target="tpu_custom_call" | custom-call | tf_op jit(solution)/shard_map/attend/pallas_call | solution.py:404
  45.2 90.4 %experts.1 = bf16[64,4096]{1,0:T(8,128)(2,1)} custom-call(bf16[8,24,4096]{2,1,0:T(8,128)(2,1)} %get-tuple-element.9.out_ref, f32[64,128]{1,0:T(8,128)} %get-tuple-element.10.meta, bf16[64,4096]{1,0:T(8,128)(2,1)} %get-tuple-element.11.x_one, f32[1,4096]{1,0:T(1,128)} %bitcast.12, bf16[4096,256]{1,0:T(8,128)(2,1)} %bitcast.9, bf16[4096,256]{1,0:T(8,128)(2,1)} %bitcast.10, ...), custom_call_target="tpu_custom_call" | custom-call | tf_op jit(solution)/shard_map/experts/pallas_call | solution.py:754
  135.6 1.9 %copy.23 = bf16[64,4096]{1,0:T(8,128)(2,1)} copy(bf16[64,4096]{1,0:T(8,128)(2,1)} %experts.1) | data formatting | bytes 1048576
  (1 shorter events, 0.0 us)
